TPU v7x, 32 devices: a whole 2x2x4 slice. The times are simulated.
32 devices in a mesh: dp: 2 (over x), kv: 8 (over z, y), tp: 2 (over core).
Axes of the slice: x: 2, y: 2, z: 4, core: 2. Of those that a mesh axis runs over, the one named last changes fastest.
Arguments:
- tokens: bfloat16 [2, 1536, 2048], P('dp', 'kv'), may hold values from -60 to 60
- doc_lengths: int32 [2, 8], P('dp'), may hold values from 1 to 768, as said below
- picked: int32 [2, 48, 32], P('dp', 'kv'), may hold values from -1 to 47, as said below
- w_query: bfloat16 [2048, 1024], P(None, 'tp'), may hold values from -0.125 to 0.125
- w_key: bfloat16 [2048, 128], replicated, may hold values from -0.125 to 0.125
- w_value: bfloat16 [2048, 128], replicated, may hold values from -0.125 to 0.125
- w_out: bfloat16 [1024, 2048], replicated, may hold values from -0.1875 to 0.1875
Outputs:
- mixed: bfloat16 [2, 1536, 2048], P('dp', 'kv')
Inputs may be any that keep to these rules, and one draw needn't show every extreme that they name: `doc_lengths`: each row sums to 1536; its largest document has exactly 768 positions. `picked`: slot 0 of query block b is b itself; the other slots hold distinct blocks before b, or -1 when fewer such blocks are named. Of the 6 blocks that one device of kv holds, at most 2 are named by query blocks held by other devices of kv, and in every row some device reaches 2.
All inputs are finite; a program needn't handle non-finite values.
Results may differ from a plain program's by a relative error of at most 0.011.
Values may be sent and summed in bfloat16 or wider, within the bound.
A program may use at most 64 MiB of HBM per device.

v0:
```python
import jax
import jax.numpy as jnp
from jax import lax
from jax.sharding import PartitionSpec as P

KV_HEADS = 2
HEAD_DIM = 64
BLOCK = 32
PICKS = 32


def rotate(values_in, positions):
    half = values_in.shape[-1] // 2
    inverse = 10000.0 ** (-jnp.arange(half, dtype=jnp.float32) / half)
    angles = positions.astype(jnp.float32)[:, None] * inverse[None, :]
    cosine = jnp.cos(angles)[:, None, :]
    sine = jnp.sin(angles)[:, None, :]
    first = values_in[..., :half]
    second = values_in[..., half:]
    return jnp.concatenate(
        [first * cosine - second * sine, second * cosine + first * sine], axis=-1
    )


def doc_of(positions, ends):
    return jnp.sum((positions[..., None] >= ends).astype(jnp.int32), axis=-1)


def shards(tokens, doc_lengths, picked, w_query, w_key, w_value, w_out):
    local = tokens[0]
    rows = local.shape[0]
    kv_index = lax.axis_index("kv")
    tp_index = lax.axis_index("tp")
    positions = kv_index * rows + jnp.arange(rows, dtype=jnp.int32)
    heads_dev = w_query.shape[1] // HEAD_DIM
    kv_dev = KV_HEADS // lax.axis_size("tp")
    group = heads_dev // kv_dev
    width = kv_dev * HEAD_DIM
    queries = rotate(
        jnp.dot(local, w_query, preferred_element_type=jnp.float32).reshape(
            rows, heads_dev, HEAD_DIM
        ),
        positions,
    ).astype(jnp.bfloat16)
    key_cols = lax.dynamic_slice_in_dim(w_key, tp_index * width, width, 1)
    value_cols = lax.dynamic_slice_in_dim(w_value, tp_index * width, width, 1)
    keys = rotate(
        jnp.dot(local, key_cols, preferred_element_type=jnp.float32).reshape(
            rows, kv_dev, HEAD_DIM
        ),
        positions,
    ).astype(jnp.bfloat16)
    values = jnp.dot(local, value_cols, preferred_element_type=jnp.float32).astype(jnp.bfloat16)
    packed = jnp.concatenate([keys.reshape(rows, width), values], axis=1)
    ends = jnp.cumsum(doc_lengths[0])
    blocks_dev = rows // BLOCK
    slots = picked[0]
    offsets = jnp.arange(BLOCK, dtype=jnp.int32)
    chosen = jnp.maximum(slots, 0)
    key_pos = (chosen[:, :, None] * BLOCK + offsets[None, None, :]).reshape(
        blocks_dev, PICKS * BLOCK
    )
    every = lax.all_gather(packed, "kv", axis=0, tiled=True)
    selected = every[key_pos]
    block_keys = selected[..., :width].reshape(blocks_dev, PICKS * BLOCK, kv_dev, HEAD_DIM)
    block_values = selected[..., width:].reshape(blocks_dev, PICKS * BLOCK, kv_dev, HEAD_DIM)
    query_pos = positions.reshape(blocks_dev, BLOCK)
    filled = jnp.repeat(slots >= 0, BLOCK, axis=1)
    live = (
        filled[:, None, :]
        & (key_pos[:, None, :] <= query_pos[:, :, None])
        & (doc_of(key_pos, ends)[:, None, :] == doc_of(query_pos, ends)[:, :, None])
    )
    grouped = queries.reshape(blocks_dev, BLOCK, kv_dev, group, HEAD_DIM)
    scores = jnp.einsum(
        "bqngd,bknd->bngqk", grouped, block_keys, preferred_element_type=jnp.float32
    ) * HEAD_DIM ** (-0.5)
    scores = jnp.where(live[:, None, None], scores, -jnp.inf)
    highest = jnp.max(scores, axis=-1, keepdims=True)
    weights = jnp.exp(scores - highest)
    total = jnp.sum(weights, axis=-1)
    summed = jnp.einsum(
        "bngqk,bknd->bqngd",
        weights.astype(jnp.bfloat16),
        block_values,
        preferred_element_type=jnp.float32,
    )
    result = summed / jnp.transpose(total, (0, 3, 1, 2))[..., None]
    attended = result.astype(jnp.bfloat16).reshape(rows, heads_dev * HEAD_DIM)
    whole = lax.all_gather(attended, "tp", axis=1, tiled=True)
    mixed = jnp.dot(whole, w_out, preferred_element_type=jnp.float32).astype(jnp.bfloat16)
    return mixed[None]


def solution(mesh):
    placed = (P("dp", "kv", None), P("dp", None), P("dp", "kv", None), P(None, "tp"), P(), P(), P())
    return jax.shard_map(
        shards, mesh=mesh, in_specs=placed, out_specs=P("dp", "kv", None), check_vma=False
    )
```

profile of v0, /device:TPU:0, one launch (start us, length us, event | category | flops | bytes accessed | tf_op | source)
XLA Modules:
  0.0 83.3 jit_solution(2517462831864149929)
XLA Ops:
  0.0 0.9 %reduce-window.8 = s32[8,1]{0,1:T(1,128)S(1)} reduce-window(s32[8,1]{0,1:T(1,128)} %bitcast.114, s32[]{:T(128)} %constant.13.clone.1), window={size=8x1 pad=7_0x0_0}, to_apply=%region_0.0 | reduce-window | flops 56 | bytes 68 | tf_op jit(solution)/shard_map/reduce-window.3
  0.9 0.7 broadcast_compare_fusion
  1.6 0.7 maximum_multiply_fusion
  2.7 1.7 %fusion.15 = bf16[192,64]{0,1:T(8,128)(2,1)S(1)} fusion(bf16[1,192,2048]{2,1,0:T(8,128)(2,1)S(1)} %copy-done, bf16[2048,128]{1,0:T(8,128)(2,1)} %param.12, s32[]{:T(128)S(6)} %select_n.18), kind=kOutput, calls=%fused_computation.20 | convolution fusion | flops 50343936 | bytes 1335300 | tf_op jit(solution)/shard_map/dot_general | solution.py:53
  4.4 1.6 %convolution_bitcast_fusion = f32[192,1,64]{0,2,1:T(8,128)S(1)} fusion(bf16[1,192,2048]{2,1,0:T(8,128)(2,1)S(1)} %copy-done, bf16[2048,128]{1,0:T(8,128)(2,1)} %param.11, s32[]{:T(128)S(6)} %select_n.18), kind=kOutput, calls=%fused_computation.18 | convolution fusion | flops 50331648 | bytes 1359876 | tf_op jit(solution)/shard_map/dot_general | solution.py:48
  6.1 0.2 fusion.40
  6.4 0.8 multiply_cosine_fusion
  7.6 0.1 convert_reduce_fusion
  7.7 0.4 compare_and_fusion
  8.1 32.8 %all_gather.6 = bf16[1536,128]{1,0:T(8,128)(2,1)S(1)} all-gather(bf16[192,128]{1,0:T(8,128)(2,1)S(1)} %copy.26), channel_id=1, replica_groups=mesh['dp'=2,'kv'=8,'tp'=2] {'kv'}, dimensions={0}, use_global_device_ids=true | all-gather | bytes 442368 | tf_op jit(solution)/shard_map/all_gather | solution.py:63
  40.9 22.0 %gather_fusion = bf16[6144,128]{1,0:T(8,128)(2,1)} fusion(bf16[1536,128]{1,0:T(8,128)(2,1)S(1)} %all_gather.6, s32[6144]{0:T(1024)S(1)} %broadcast_clamp_fusion), kind=kCustom, calls=%fused_computation | custom fusion | bytes 3170304 | tf_op jit(solution)/shard_map/gather | solution.py:64
  62.9 2.5 %copy.29 = bf16[2048,512]{0,1:T(8,128)(2,1)} copy(bf16[2048,512]{1,0:T(8,128)(2,1)S(1)} %copy-done.1) | data formatting | bytes 4194304 | tf_op args[3]
  65.4 2.4 %fusion.22 = f32[192,8,64]{0,2,1:T(8,128)S(1)} fusion(bf16[8,64,2048]{2,1,0:T(8,128)(2,1)} %bitcast.106, bf16[1,192,2048]{2,1,0:T(8,128)(2,1)S(1)} %copy-done), kind=kOutput, calls=%fused_computation.23 | convolution fusion | flops 402653184 | bytes 3276800 | tf_op jit(solution)/shard_map/dot_general | solution.py:40
  67.9 0.3 concatenate.26
  68.2 1.1 %copy.30 = bf16[6,32,8,32]{3,1,2,0:T(8,128)(2,1)} copy(bf16[6,32,8,32]{1,0,3,2:T(8,128)(2,1)S(1)} %concatenate.26) | data formatting | bytes 196608 | tf_op jit(solution)/shard_map/concatenate | solution.py:20
  69.3 0.3 concatenate.27
  69.5 1.1 %copy.31 = bf16[6,32,8,32]{3,1,2,0:T(8,128)(2,1)} copy(bf16[6,32,8,32]{1,0,3,2:T(8,128)(2,1)S(1)} %concatenate.27) | data formatting | bytes 196608 | tf_op jit(solution)/shard_map/concatenate | solution.py:20
  70.6 2.3 %fusion.2 = (f32[6,8,32]{2,1,0:T(8,128)S(1)}, f32[6,1024,32,8]{1,2,3,0:T(8,128)S(1)}) fusion(pred[6,32,1024]{2,1,0:T(8,128)(4,1)S(1)} %compare_and_fusion, bf16[6,32,8,32]{3,1,2,0:T(8,128)(2,1)} %copy.31, bf16[6,32,8,32]{3,1,2,0:T(8,128)(2,1)} %copy.30, bf16[6,1024,128]{2,1,0:T(8,128)(2,1)S(1)} %bitcast.107), kind=kOutput, calls=%fused_computation.5 | convolution fusion | flops 206436864 | bytes 8263680 | tf_op jit(solution)/shard_map/bqngd,bknd->bngqk/dot_general | solution.py:75
  72.9 1.6 %fusion = f32[6,8,32]{2,1,0:T(8,128)S(1)} fusion(f32[6,1024,32,8]{1,2,3,0:T(8,128)S(1)} %get-tuple-element.12, f32[6,8,32]{2,1,0:T(8,128)S(1)} %get-tuple-element.11, pred[6,32,1024]{2,1,0:T(8,128)(4,1)S(1)} %compare_and_fusion), kind=kLoop, calls=%fused_computation.3 | loop fusion | flops 6289920 | bytes 6500352 | tf_op jit(solution)/shard_map/reduce_sum | solution.py:81
  74.6 2.1 %fusion.19 = bf16[6,32,1,8,64]{4,1,3,0,2:T(8,128)(2,1)S(1)} fusion(f32[6,1024,32,8]{1,2,3,0:T(8,128)S(1)} %get-tuple-element.12, f32[6,8,32]{2,1,0:T(8,128)S(1)} %get-tuple-element.11, pred[6,32,1024]{2,1,0:T(8,128)(4,1)S(1)} %compare_and_fusion, bf16[6,1024,128]{2,1,0:T(8,128)(2,1)S(1)} %bitcast.108, f32[6,32,8]{1,2,0:T(8,128)S(1)} %bitcast.109), kind=kOutput, calls=%fused_computation.22 | convolution fusion | flops 207814656 | bytes 8269824 | tf_op jit(solution)/shard_map/bngqk,bknd->bqngd/dot_general | solution.py:82
  76.7 0.2 copy.32
  76.9 0.3 reshape.293
  77.1 2.1 %all_gather.7 = bf16[192,1024]{1,0:T(8,128)(2,1)S(1)} all-gather(bf16[192,512]{1,0:T(8,128)(2,1)S(1)} %reshape.293), channel_id=1, replica_groups=mesh['dp'=2,'kv'=8,'tp'=2] {'tp'}, dimensions={1}, use_global_device_ids=true | all-gather | bytes 589824 | tf_op jit(solution)/shard_map/all_gather | solution.py:90
  79.2 4.1 %fusion.10 = bf16[1,192,2048]{2,1,0:T(8,128)(2,1)} fusion(bf16[192,1024]{1,0:T(8,128)(2,1)S(1)} %all_gather.7, bf16[1024,2048]{1,0:T(8,128)(2,1)} %param.13), kind=kOutput, calls=%fused_computation.13 | convolution fusion | flops 805699584 | bytes 5373952 | tf_op jit(solution)/shard_map/dot_general | solution.py:91
  (28 shorter events, 0.9 us)
Async XLA Ops:
  0.0 2.7 %copy-start = (bf16[1,192,2048]{2,1,0:T(8,128)(2,1)S(1)}, bf16[1,192,2048]{2,1,0:T(8,128)(2,1)}, u32[]{:S(2)}) copy-start(bf16[1,192,2048]{2,1,0:T(8,128)(2,1)} %param.7) | copy-start | bytes 2359300
  40.9 22.0 %copy-start.1 = (bf16[2048,512]{1,0:T(8,128)(2,1)S(1)}, bf16[2048,512]{1,0:T(8,128)(2,1)}, u32[]{:S(2)}) copy-start(bf16[2048,512]{1,0:T(8,128)(2,1)} %param.10) | copy-start | bytes 6291460
  62.9 4.9 %copy-start.3 = (f32[192,32]{0,1:T(8,128)S(1)}, f32[192,32]{0,1:T(8,128)}, u32[]{:S(2)}) copy-start(f32[192,32]{0,1:T(8,128)} %get-tuple-element.10) | copy-start | bytes 73732
  65.4 5.2 %copy-start.2 = (bf16[6144,128]{1,0:T(8,128)(2,1)S(1)}, bf16[6144,128]{1,0:T(8,128)(2,1)}, u32[]{:S(2)}) copy-start(bf16[6144,128]{1,0:T(8,128)(2,1)} %gather_fusion) | copy-start | bytes 4718596
where the time goes:
time: 83.7 us; the launch traced here: 83.3 us
  blocking collectives  34.9 us (42%)
  local copies, waits for them, and re-layouts  28.3 us (34%)
  matrix products  14.3 us (17%)
  other arithmetic  5.67 us (7%)
    all_gather x1, blocking collectives, shards(): every = lax.all_gather(packed, 'kv', axis=0, tiled=True)  32.8 us
    gather x1, local copies, waits for them, and re-layouts, shards(): selected = every[key_pos]  22 us
    dot_general x1, matrix products, shards(): jnp.dot(whole, w_out, preferred_element_type=jnp.float32)  4.07 us
    concatenate x4, local copies, waits for them, and re-layouts, rotate(): jnp.concatenate([first * cosine - second * sine, second * cosine + first...  2.67 us
    unnamed x11, local copies, waits for them, and re-layouts  2.5 us
    dot_general x1, matrix products, shards(): jnp.dot(local, w_query, preferred_element_type=jnp.float32)  2.44 us
    dot_general x1, matrix products, shards(): jnp.einsum('bqngd,bknd->bngqk', grouped, block_keys, preferred_element_ty...  2.3 us
    dot_general x1, matrix products, shards(): jnp.einsum('bngqk,bknd->bqngd', weights.astype(jnp.bfloat16), block_value...  2.13 us

commit v1 on v0

--- a/solution.py
+++ b/solution.py
@@ -7,6 +7,16 @@
 HEAD_DIM = 64
 BLOCK = 32
 PICKS = 32
+
+
+def turned_line(shard, axis, dim):
+    peers = lax.axis_size(axis)
+    held, parts = (shard, [shard])
+    for _ in range(peers - 1):
+        held = lax.ppermute(held, axis, [(i, (i + 1) % peers) for i in range(peers)])
+        parts.insert(0, held)
+    merged = jnp.concatenate(parts, axis=dim)
+    return jnp.roll(merged, (lax.axis_index(axis) + 1) * shard.shape[dim], axis=dim)
 
 
 def rotate(values_in, positions):
@@ -60,7 +70,7 @@
     key_pos = (chosen[:, :, None] * BLOCK + offsets[None, None, :]).reshape(
         blocks_dev, PICKS * BLOCK
     )
-    every = lax.all_gather(packed, "kv", axis=0, tiled=True)
+    every = turned_line(packed, "kv", 0)
     selected = every[key_pos]
     block_keys = selected[..., :width].reshape(blocks_dev, PICKS * BLOCK, kv_dev, HEAD_DIM)
     block_values = selected[..., width:].reshape(blocks_dev, PICKS * BLOCK, kv_dev, HEAD_DIM)

time: 83.7 us -> 88.4 us (1.056)
  waiting for transfers between devices: 0 us -> 37.1 us
  blocking collectives: 34.9 us -> 2.09 us
  starting transfers between devices: 0 us -> 4.58 us
  local copies, waits for them, and re-layouts: 28.3 us -> 26.2 us
  other arithmetic: 5.67 us -> 3.63 us
    ppermute x0 -> x7, waiting for transfers between devices: none -> 37.1 us  [turned_line(): lax.ppermute(held, axis, [(i, (i + 1) % peers) for i in range(peers)])]
    all_gather x1 -> x0, blocking collectives: 32.8 us -> none  [shards(): every = lax.all_gather(packed, 'kv', axis=0, tiled=True)]
    ppermute x0 -> x7, starting transfers between devices: none -> 4.58 us  [turned_line(): lax.ppermute(held, axis, [(i, (i + 1) % peers) for i in range(peers)])]
    gather x1, local copies, waits for them, and re-layouts: 22 us -> 18.1 us  [shards(): selected = every[key_pos]]
    unnamed x11, local copies, waits for them, and re-layouts: 2.5 us -> 3.59 us
  transfers between devices with their start and end apart: 0 -> 7, of which waited for: 0 -> 6; matrix products, arithmetic and copies ran while one was open for 0% -> 11% of each run, Pallas kernels for 0% -> 0%
where the time goes in v1:
time: 88.4 us; the launch traced here: 88.1 us
  waiting for transfers between devices  37.1 us (42%)
  local copies, waits for them, and re-layouts  26.2 us (30%)
  matrix products  14.2 us (16%)
  starting transfers between devices  4.58 us (5%)
  other arithmetic  3.63 us (4%)
  blocking collectives  2.09 us (2%)
    ppermute x7, waiting for transfers between devices, turned_line(): lax.ppermute(held, axis, [(i, (i + 1) % peers) for i in range(peers)])  37.1 us
    gather x1, local copies, waits for them, and re-layouts, shards(): selected = every[key_pos]  18.1 us
    ppermute x7, starting transfers between devices, turned_line(): lax.ppermute(held, axis, [(i, (i + 1) % peers) for i in range(peers)])  4.58 us
    dot_general x1, matrix products, shards(): jnp.dot(whole, w_out, preferred_element_type=jnp.float32)  4.08 us
    unnamed x11, local copies, waits for them, and re-layouts  3.59 us
    concatenate x4, local copies, waits for them, and re-layouts, rotate(): jnp.concatenate([first * cosine - second * sine, second * cosine + first...  2.66 us
    dot_general x1, matrix products, shards(): jnp.dot(local, w_query, preferred_element_type=jnp.float32)  2.32 us
    dot_general x1, matrix products, shards(): jnp.einsum('bqngd,bknd->bngqk', grouped, block_keys, preferred_element_ty...  2.31 us
  transfers between devices with their start and end apart: 7, of which 6 were waited for; matrix products, arithmetic and copies ran while one was open for 11% of the time, Pallas kernels for 0%

profile of v1, /device:TPU:0, one launch (start us, length us, event | category | flops | bytes accessed | tf_op | source)
XLA Modules:
  0.0 88.1 jit_solution(7460922674338695233)
XLA Ops:
  0.0 1.1 %copy-done = bf16[1,192,2048]{2,1,0:T(8,128)(2,1)S(1)} copy-done((bf16[1,192,2048]{2,1,0:T(8,128)(2,1)S(1)}, bf16[1,192,2048]{2,1,0:T(8,128)(2,1)}, u32[]{:S(2)}) %copy-start) | copy-done | bytes 786456
  1.1 1.7 %fusion.15 = bf16[192,64]{0,1:T(8,128)(2,1)S(1)} fusion(bf16[1,192,2048]{2,1,0:T(8,128)(2,1)S(1)} %copy-done, bf16[2048,128]{1,0:T(8,128)(2,1)} %param.12, s32[]{:T(128)S(6)} %select_n.31), kind=kOutput, calls=%fused_computation.20 | convolution fusion | flops 50343936 | bytes 1335300 | tf_op jit(solution)/shard_map/dot_general | solution.py:63
  2.8 1.7 %convolution_bitcast_fusion = f32[192,1,64]{0,2,1:T(8,128)S(1)} fusion(bf16[1,192,2048]{2,1,0:T(8,128)(2,1)S(1)} %copy-done, bf16[2048,128]{1,0:T(8,128)(2,1)} %param.11, s32[]{:T(128)S(6)} %select_n.31), kind=kOutput, calls=%fused_computation.18 | convolution fusion | flops 50331648 | bytes 1359876 | tf_op jit(solution)/shard_map/dot_general | solution.py:58
  4.7 3.0 %collective-permute-start = (bf16[192,128]{0,1:T(8,128)(2,1)S(1)}, bf16[192,128]{0,1:T(8,128)(2,1)S(1)}, u32[]{:S(2)}, u32[]{:S(2)}) collective-permute-start(bf16[192,128]{0,1:T(8,128)(2,1)S(1)} %pad_maximum_fusion), channel_id=1, source_target_pairs={{0,2},{2,4},{4,6},{6,8},{8,10},{10,12},{12,14},{14,0},{1,3},{3,5},... | collective-permute-start | bytes 147464 | tf_op jit(solution)/shard_map/ppermute | solution.py:16
  8.0 0.7 maximum_multiply_fusion
  9.0 2.5 %copy.22 = bf16[2048,512]{0,1:T(8,128)(2,1)} copy(bf16[2048,512]{1,0:T(8,128)(2,1)S(1)} %copy-done.1) | data formatting | bytes 4194304 | tf_op args[3]
  11.4 2.3 %fusion.22 = f32[192,8,64]{0,2,1:T(8,128)S(1)} fusion(bf16[8,64,2048]{2,1,0:T(8,128)(2,1)} %bitcast.106, bf16[1,192,2048]{2,1,0:T(8,128)(2,1)S(1)} %copy-done), kind=kOutput, calls=%fused_computation.23 | convolution fusion | flops 402653184 | bytes 3276800 | tf_op jit(solution)/shard_map/dot_general | solution.py:50
  14.1 1.5 %collective-permute-start.1 = (bf16[192,128]{0,1:T(8,128)(2,1)S(1)}, bf16[192,128]{0,1:T(8,128)(2,1)S(1)}, u32[]{:S(2)}, u32[]{:S(2)}) collective-permute-start(bf16[192,128]{0,1:T(8,128)(2,1)S(1)} %collective-permute-done), channel_id=1, source_target_pairs={{0,2},{2,4},{4,6},{6,8},{8,10},{10,12},{12,14},{14,0},{1,3},{3,5},... | collective-permute-start | bytes 147464 | tf_op jit(solution)/shard_map/ppermute | solution.py:16
  15.7 5.3 %collective-permute-done.1 = bf16[192,128]{0,1:T(8,128)(2,1)S(1)} collective-permute-done((bf16[192,128]{0,1:T(8,128)(2,1)S(1)}, bf16[192,128]{0,1:T(8,128)(2,1)S(1)}, u32[]{:S(2)}, u32[]{:S(2)}) %collective-permute-start.1) | collective-permute-done | bytes 49184 | tf_op jit(solution)/shard_map/ppermute | solution.py:16
  21.0 7.0 %collective-permute-done.2 = bf16[192,128]{0,1:T(8,128)(2,1)S(1)} collective-permute-done((bf16[192,128]{0,1:T(8,128)(2,1)S(1)}, bf16[192,128]{0,1:T(8,128)(2,1)S(1)}, u32[]{:S(2)}, u32[]{:S(2)}) %collective-permute-start.2) | collective-permute-done | bytes 49184 | tf_op jit(solution)/shard_map/ppermute | solution.py:16
  28.3 6.6 %collective-permute-done.3 = bf16[192,128]{0,1:T(8,128)(2,1)S(1)} collective-permute-done((bf16[192,128]{0,1:T(8,128)(2,1)S(1)}, bf16[192,128]{0,1:T(8,128)(2,1)S(1)}, u32[]{:S(2)}, u32[]{:S(2)}) %collective-permute-start.3) | collective-permute-done | bytes 49184 | tf_op jit(solution)/shard_map/ppermute | solution.py:16
  35.0 0.4 compare_and_fusion
  35.4 6.5 %collective-permute-done.4 = bf16[192,128]{0,1:T(8,128)(2,1)S(1)} collective-permute-done((bf16[192,128]{0,1:T(8,128)(2,1)S(1)}, bf16[192,128]{0,1:T(8,128)(2,1)S(1)}, u32[]{:S(2)}, u32[]{:S(2)}) %collective-permute-start.4) | collective-permute-done | bytes 49184 | tf_op jit(solution)/shard_map/ppermute | solution.py:16
  42.0 7.4 %collective-permute-done.5 = bf16[192,128]{0,1:T(8,128)(2,1)S(1)} collective-permute-done((bf16[192,128]{0,1:T(8,128)(2,1)S(1)}, bf16[192,128]{0,1:T(8,128)(2,1)S(1)}, u32[]{:S(2)}, u32[]{:S(2)}) %collective-permute-start.5) | collective-permute-done | bytes 49184 | tf_op jit(solution)/shard_map/ppermute | solution.py:16
  49.7 1.1 %copy.23 = bf16[6,32,8,32]{3,1,2,0:T(8,128)(2,1)} copy(bf16[6,32,8,32]{1,0,3,2:T(8,128)(2,1)S(1)} %concatenate.33) | data formatting | bytes 196608 | tf_op jit(solution)/shard_map/concatenate | solution.py:30
  51.0 1.1 %copy.24 = bf16[6,32,8,32]{3,1,2,0:T(8,128)(2,1)} copy(bf16[6,32,8,32]{1,0,3,2:T(8,128)(2,1)S(1)} %concatenate.34) | data formatting | bytes 196608 | tf_op jit(solution)/shard_map/concatenate | solution.py:30
  52.1 4.2 %collective-permute-done.6 = bf16[192,128]{0,1:T(8,128)(2,1)S(1)} collective-permute-done((bf16[192,128]{0,1:T(8,128)(2,1)S(1)}, bf16[192,128]{0,1:T(8,128)(2,1)S(1)}, u32[]{:S(2)}, u32[]{:S(2)}) %collective-permute-start.6) | collective-permute-done | bytes 49184 | tf_op jit(solution)/shard_map/ppermute | solution.py:16
  56.4 0.5 concatenate.32
  57.3 18.1 %gather_fusion = bf16[6144,128]{1,0:T(8,128)(2,1)S(1)} fusion(bf16[1536,128]{1,0:T(8,128)(2,1)S(1)} %copy.19, s32[6144]{0:T(1024)S(1)} %broadcast_clamp_fusion), kind=kCustom, calls=%fused_computation | custom fusion | bytes 3170304 | tf_op jit(solution)/shard_map/gather | solution.py:74
  75.4 2.3 %fusion.2 = (f32[6,8,32]{2,1,0:T(8,128)S(1)}, f32[6,1024,32,8]{1,2,3,0:T(8,128)S(1)}) fusion(pred[6,32,1024]{2,1,0:T(8,128)(4,1)S(1)} %compare_and_fusion, bf16[6,32,8,32]{3,1,2,0:T(8,128)(2,1)} %copy.24, bf16[6,32,8,32]{3,1,2,0:T(8,128)(2,1)} %copy.23, bf16[6,1024,128]{2,1,0:T(8,128)(2,1)S(1)} %bitcast.107), kind=kOutput, calls=%fused_computation.5 | convolution fusion | flops 206436864 | bytes 8263680 | tf_op jit(solution)/shard_map/bqngd,bknd->bngqk/dot_general | solution.py:85
  77.7 1.6 %fusion = f32[6,8,32]{2,1,0:T(8,128)S(1)} fusion(f32[6,1024,32,8]{1,2,3,0:T(8,128)S(1)} %get-tuple-element.12, f32[6,8,32]{2,1,0:T(8,128)S(1)} %get-tuple-element.11, pred[6,32,1024]{2,1,0:T(8,128)(4,1)S(1)} %compare_and_fusion), kind=kLoop, calls=%fused_computation.3 | loop fusion | flops 6289920 | bytes 6500352 | tf_op jit(solution)/shard_map/reduce_sum | solution.py:91
  79.3 2.1 %fusion.19 = bf16[6,32,1,8,64]{4,1,3,0,2:T(8,128)(2,1)S(1)} fusion(f32[6,1024,32,8]{1,2,3,0:T(8,128)S(1)} %get-tuple-element.12, f32[6,8,32]{2,1,0:T(8,128)S(1)} %get-tuple-element.11, pred[6,32,1024]{2,1,0:T(8,128)(4,1)S(1)} %compare_and_fusion, bf16[6,1024,128]{2,1,0:T(8,128)(2,1)S(1)} %bitcast.108, f32[6,32,8]{1,2,0:T(8,128)S(1)} %bitcast.109), kind=kOutput, calls=%fused_computation.22 | convolution fusion | flops 207814656 | bytes 8269824 | tf_op jit(solution)/shard_map/bngqk,bknd->bqngd/dot_general | solution.py:92
  81.9 2.1 %all_gather.3 = bf16[192,1024]{1,0:T(8,128)(2,1)S(1)} all-gather(bf16[192,512]{1,0:T(8,128)(2,1)S(1)} %reshape.293), channel_id=1, replica_groups=mesh['dp'=2,'kv'=8,'tp'=2] {'tp'}, dimensions={1}, use_global_device_ids=true | all-gather | bytes 589824 | tf_op jit(solution)/shard_map/all_gather | solution.py:100
  84.0 4.1 %fusion.10 = bf16[1,192,2048]{2,1,0:T(8,128)(2,1)} fusion(bf16[192,1024]{1,0:T(8,128)(2,1)S(1)} %all_gather.3, bf16[1024,2048]{1,0:T(8,128)(2,1)} %param.13), kind=kOutput, calls=%fused_computation.13 | convolution fusion | flops 805699584 | bytes 5373952 | tf_op jit(solution)/shard_map/dot_general | solution.py:101
  (43 shorter events, 2.9 us)
Async XLA Ops:
  0.0 1.1 %copy-start = (bf16[1,192,2048]{2,1,0:T(8,128)(2,1)S(1)}, bf16[1,192,2048]{2,1,0:T(8,128)(2,1)}, u32[]{:S(2)}) copy-start(bf16[1,192,2048]{2,1,0:T(8,128)(2,1)} %param.7) | copy-start | bytes 2359300
  0.0 8.9 %copy-start.1 = (bf16[2048,512]{1,0:T(8,128)(2,1)S(1)}, bf16[2048,512]{1,0:T(8,128)(2,1)}, u32[]{:S(2)}) copy-start(bf16[2048,512]{1,0:T(8,128)(2,1)} %param.10) | copy-start | bytes 6291460
  4.7 9.3 %collective-permute-start = (bf16[192,128]{0,1:T(8,128)(2,1)S(1)}, bf16[192,128]{0,1:T(8,128)(2,1)S(1)}, u32[]{:S(2)}, u32[]{:S(2)}) collective-permute-start(bf16[192,128]{0,1:T(8,128)(2,1)S(1)} %pad_maximum_fusion), channel_id=1, source_target_pairs={{0,2},{2,4},{4,6},{6,8},{8,10},{10,12},{12,14},{14,0},{1,3},{3,5},... | collective-permute-start | bytes 147464 | tf_op jit(solution)/shard_map/ppermute | solution.py:16
  8.9 4.9 %copy-start.2 = (s32[1,6,32]{2,0,1:T(1,128)S(1)}, s32[1,6,32]{2,0,1:T(1,128)}, u32[]{:S(2)}) copy-start(s32[1,6,32]{2,0,1:T(1,128)} %param.9) | copy-start | bytes 2308
  9.0 4.9 %copy-start.3 = (s32[1,8]{1,0:T(1,128)S(1)}, s32[1,8]{1,0:T(1,128)}, u32[]{:S(2)}) copy-start(s32[1,8]{1,0:T(1,128)} %param.8) | copy-start | bytes 100
  14.1 7.0 %collective-permute-start.1 = (bf16[192,128]{0,1:T(8,128)(2,1)S(1)}, bf16[192,128]{0,1:T(8,128)(2,1)S(1)}, u32[]{:S(2)}, u32[]{:S(2)}) collective-permute-start(bf16[192,128]{0,1:T(8,128)(2,1)S(1)} %collective-permute-done), channel_id=1, source_target_pairs={{0,2},{2,4},{4,6},{6,8},{8,10},{10,12},{12,14},{14,0},{1,3},{3,5},... | collective-permute-start | bytes 147464 | tf_op jit(solution)/shard_map/ppermute | solution.py:16
  21.0 7.0 %collective-permute-start.2 = (bf16[192,128]{0,1:T(8,128)(2,1)S(1)}, bf16[192,128]{0,1:T(8,128)(2,1)S(1)}, u32[]{:S(2)}, u32[]{:S(2)}) collective-permute-start(bf16[192,128]{0,1:T(8,128)(2,1)S(1)} %collective-permute-done.1), channel_id=1, source_target_pairs={{0,2},{2,4},{4,6},{6,8},{8,10},{10,12},{12,14},{14,0},{1,3},{3,5},... | collective-permute-start | bytes 147464 | tf_op jit(solution)/shard_map/ppermute | solution.py:16
  28.0 7.0 %collective-permute-start.3 = (bf16[192,128]{0,1:T(8,128)(2,1)S(1)}, bf16[192,128]{0,1:T(8,128)(2,1)S(1)}, u32[]{:S(2)}, u32[]{:S(2)}) collective-permute-start(bf16[192,128]{0,1:T(8,128)(2,1)S(1)} %collective-permute-done.2), channel_id=1, source_target_pairs={{0,2},{2,4},{4,6},{6,8},{8,10},{10,12},{12,14},{14,0},{1,3},{3,5},... | collective-permute-start | bytes 147464 | tf_op jit(solution)/shard_map/ppermute | solution.py:16
  35.0 7.0 %collective-permute-start.4 = (bf16[192,128]{0,1:T(8,128)(2,1)S(1)}, bf16[192,128]{0,1:T(8,128)(2,1)S(1)}, u32[]{:S(2)}, u32[]{:S(2)}) collective-permute-start(bf16[192,128]{0,1:T(8,128)(2,1)S(1)} %collective-permute-done.3), channel_id=1, source_target_pairs={{0,2},{2,4},{4,6},{6,8},{8,10},{10,12},{12,14},{14,0},{1,3},{3,5},... | collective-permute-start | bytes 147464 | tf_op jit(solution)/shard_map/ppermute | solution.py:16
  41.9 7.5 %collective-permute-start.5 = (bf16[192,128]{0,1:T(8,128)(2,1)S(1)}, bf16[192,128]{0,1:T(8,128)(2,1)S(1)}, u32[]{:S(2)}, u32[]{:S(2)}) collective-permute-start(bf16[192,128]{0,1:T(8,128)(2,1)S(1)} %collective-permute-done.4), channel_id=1, source_target_pairs={{0,2},{2,4},{4,6},{6,8},{8,10},{10,12},{12,14},{14,0},{1,3},{3,5},... | collective-permute-start | bytes 147464 | tf_op jit(solution)/shard_map/ppermute | solution.py:16
  49.4 7.0 %collective-permute-start.6 = (bf16[192,128]{0,1:T(8,128)(2,1)S(1)}, bf16[192,128]{0,1:T(8,128)(2,1)S(1)}, u32[]{:S(2)}, u32[]{:S(2)}) collective-permute-start(bf16[192,128]{0,1:T(8,128)(2,1)S(1)} %collective-permute-done.5), channel_id=1, source_target_pairs={{0,2},{2,4},{4,6},{6,8},{8,10},{10,12},{12,14},{14,0},{1,3},{3,5},... | collective-permute-start | bytes 147464 | tf_op jit(solution)/shard_map/ppermute | solution.py:16
